TPU v7x, 32 devices: a whole 2x2x4 slice. The times are simulated.
32 devices in a mesh: grp: 2 (over y), sp: 4 (over z), tp: 4 (over x, core).
Axes of the slice: x: 2, y: 2, z: 4, core: 2. Of those that a mesh axis runs over, the one named last changes fastest.
Arguments:
- starting_stream: bfloat16 [3072, 2048], P(('grp', 'sp'), 'tp'), parts along dimension 0, may hold values from -45 to 45
- multiplier_matrix: bfloat16 [2, 2048, 2048], P(None, 'sp', 'tp'), may hold values from -0.125 to 0.125
- memory_path_matrix: bfloat16 [2, 2048, 2048], P(None, 'sp', 'tp'), may hold values from -0.125 to 0.125
- filter_coefficients: bfloat16 [2, 4, 2048], P(None, None, 'tp'), may hold values from -3 to 3
- memory_valve_matrix: bfloat16 [2, 8, 256, 256], P(None, 'tp'), may hold values from -0.375 to 0.375
- entry_valve_matrix: bfloat16 [2, 8, 256, 256], P(None, 'tp'), may hold values from -0.375 to 0.375
- forgetting_parameters: float32 [2, 2048], P(None, 'tp'), may hold values from 3 to 15
- timestep_forgetting_multiplier: float32 [3072], P(('grp', 'sp')), parts along dimension 0, may hold values from 0.5 to 2
- spike_extra: float32 [3072, 2048], P(('grp', 'sp'), 'tp'), parts along dimension 0, may hold values from -0.7 to 0
- exit_projector_matrix: bfloat16 [2, 2048, 2048], P(None, 'tp', 'sp'), may hold values from -0.125 to 0.125
- prelude_rms_gains: float32 [2, 2048], replicated, may hold values from 0.1 to 1.9
- finishing_rms_gains: float32 [2048], P('tp'), may hold values from 0.1 to 1.9
Outputs:
- result: bfloat16 [3072, 2048], P(('grp', 'sp'), 'tp'), parts along dimension 0
There are 2 independent parts, one for each index of `grp`. A program takes and returns all parts, laid end to end along the dimension named above; an argument that names none is the same for every part. Nothing has to cross between parts.
All inputs are finite; a program needn't handle non-finite values.
Results may differ from a plain program's by a relative error of at most 0.015.
Values may be sent and summed in bfloat16 or wider, within the bound.
A program may use at most 64 MiB of HBM per device.

v0:
```python
import jax
import jax.numpy as jnp
from jax import lax
from jax.sharding import PartitionSpec as P

BLOCK_W = 256
EPSILON = 1e-06
SQUASH_POWER = 8.0


def from_behind(value, axis, steps):
    count = lax.axis_size(axis)
    first, last = (max(0, -steps), min(count, count - steps))
    return lax.ppermute(value, axis, [(source, source + steps) for source in range(first, last)])


def entering(part, axis, combine, identity):
    place = lax.axis_index(axis)
    gathered = jax.tree.map(lambda a: lax.all_gather(a, axis), part)
    state = jax.tree.map(lambda a, e: jnp.zeros_like(a) + jnp.asarray(e, a.dtype), part, identity)

    def one(lap, state):
        return combine(
            state, jax.tree.map(lambda a: lax.dynamic_index_in_dim(a, lap, 0, False), gathered)
        )

    return lax.fori_loop(0, place, one, state)


def combine_pairs(earlier, later):
    return (earlier[0] * later[0], later[0] * earlier[1] + later[1])


def gather_rows(own_cols):
    return lax.all_gather(own_cols, "tp", axis=1, tiled=True)


def on_device(
    starting_stream,
    multiplier_matrix,
    memory_path_matrix,
    filter_coefficients,
    memory_valve_matrix,
    entry_valve_matrix,
    forgetting_parameters,
    timestep_forgetting_multiplier,
    spike_extra,
    exit_projector_matrix,
    prelude_rms_gains,
    finishing_rms_gains,
):
    tok_rows = starting_stream.shape[0]
    channels = memory_path_matrix.shape[2]
    own_cols = starting_stream
    full_rows = gather_rows(starting_stream)
    for tier_number in range(memory_path_matrix.shape[0]):
        floats = full_rows.astype(jnp.float32)
        mean_square = jnp.mean(floats * floats, axis=1, keepdims=True)
        normed = (
            floats * lax.rsqrt(mean_square + EPSILON) * prelude_rms_gains[tier_number][None, :]
        ).astype(jnp.bfloat16)
        branch_acc = jnp.dot(
            normed,
            lax.all_gather(multiplier_matrix[tier_number], "sp", axis=0, tiled=True),
            preferred_element_type=jnp.float32,
        )
        recur_acc = jnp.dot(
            normed,
            lax.all_gather(memory_path_matrix[tier_number], "sp", axis=0, tiled=True),
            preferred_element_type=jnp.float32,
        )
        branch = branch_acc.astype(jnp.bfloat16)
        recurrent = recur_acc.astype(jnp.bfloat16)
        taps_now = filter_coefficients[tier_number]
        reach_back = taps_now.shape[0] - 1
        halo_rows = from_behind(recurrent[tok_rows - reach_back :], "sp", 1)
        extended = jnp.concatenate([halo_rows, recurrent], axis=0)
        conv_sum = jnp.zeros((tok_rows, channels), jnp.float32)
        for offset in range(taps_now.shape[0]):
            conv_sum = conv_sum + extended[offset : offset + tok_rows].astype(
                jnp.float32
            ) * taps_now[offset].astype(jnp.float32)
        convolved = conv_sum.astype(jnp.bfloat16)
        blocks = convolved.reshape(tok_rows, channels // BLOCK_W, BLOCK_W)
        reset_gate = jax.nn.sigmoid(
            jnp.einsum(
                "tnc,ncd->tnd",
                blocks,
                memory_valve_matrix[tier_number],
                preferred_element_type=jnp.float32,
            ).reshape(tok_rows, channels)
        )
        inject = jax.nn.sigmoid(
            jnp.einsum(
                "tnc,ncd->tnd",
                blocks,
                entry_valve_matrix[tier_number],
                preferred_element_type=jnp.float32,
            ).reshape(tok_rows, channels)
        )
        logarithmic_persistence = (
            -SQUASH_POWER
            * reset_gate
            * jax.nn.softplus(-forgetting_parameters[tier_number])[None, :]
            * timestep_forgetting_multiplier[:, None]
            + spike_extra
        )
        keep_rate = jnp.exp(logarithmic_persistence)
        driven = (
            inject
            * convolved.astype(jnp.float32)
            * jnp.sqrt(-jnp.expm1(2.0 * logarithmic_persistence))
        )
        keep_cum, state_local = lax.associative_scan(combine_pairs, (keep_rate, driven), axis=0)
        identity = (jnp.ones((channels,), jnp.float32), jnp.zeros((channels,), jnp.float32))
        carried = entering((keep_cum[-1], state_local[-1]), "sp", combine_pairs, identity)
        state_seq = state_local + keep_cum * carried[1][None, :]
        mixed_in = (jax.nn.gelu(branch.astype(jnp.float32)) * state_seq).astype(jnp.bfloat16)
        partial_value = jnp.dot(
            mixed_in,
            lax.all_gather(exit_projector_matrix[tier_number], "sp", axis=1, tiled=True),
            preferred_element_type=jnp.float32,
        )
        mixed_sum = lax.psum_scatter(
            partial_value.astype(jnp.bfloat16), "tp", scatter_dimension=1, tiled=True
        ).astype(jnp.float32)
        own_cols = (own_cols.astype(jnp.float32) + mixed_sum).astype(jnp.bfloat16)
        if tier_number + 1 < memory_path_matrix.shape[0]:
            full_rows = gather_rows(own_cols)
    floats = own_cols.astype(jnp.float32)
    full_width = floats.shape[1] * lax.axis_size("tp")
    square_sum = lax.psum(jnp.sum(floats * floats, axis=1), "tp")
    inv_rms = lax.rsqrt(square_sum / full_width + EPSILON)
    return (floats * inv_rms[:, None] * finishing_rms_gains[None, :]).astype(jnp.bfloat16)


def solution(mesh):
    return jax.shard_map(
        on_device,
        mesh=mesh,
        in_specs=(
            P(("grp", "sp"), "tp"),
            P(None, "sp", "tp"),
            P(None, "sp", "tp"),
            P(None, None, "tp"),
            P(None, "tp", None, None),
            P(None, "tp", None, None),
            P(None, "tp"),
            P(("grp", "sp")),
            P(("grp", "sp"), "tp"),
            P(None, "tp", "sp"),
            P(),
            P("tp"),
        ),
        out_specs=P(("grp", "sp"), "tp"),
        check_vma=False,
    )
```

profile of v0, /device:TPU:0, one launch (start us, length us, event | category | flops | bytes accessed | tf_op | source)
XLA Modules:
  0.0 496.0 jit_solution(4783613466114738588)
XLA Ops:
  7.3 2.3 fusion.151
  13.5 17.8 %all-gather.19.cloned.1.call-done = bf16[384,2048]{1,0:T(8,128)(2,1)} async-done(((bf16[384,512]{1,0:T(8,128)(2,1)}), bf16[384,2048]{1,0:T(8,128)(2,1)}) %all-gather.19.cloned.1.call-update) | async-done | bytes 1572880 | tf_op jit(solution)/shard_map/all_gather | solution.py:35
  31.3 1.8 fusion
  33.1 45.5 %all-gather.25.cloned.1.call-done = bf16[1,2048,512]{2,1,0:T(8,128)(2,1)} async-done(((bf16[1,512,512]{2,1,0:T(8,128)(2,1)}), bf16[1,2048,512]{2,1,0:T(8,128)(2,1)}) %all-gather.25.cloned.1.call-update) | async-done | bytes 2097168 | tf_op jit(solution)/shard_map/all_gather | solution.py:69
  78.5 3.1 fusion.31
  81.7 2.1 collective-permute-start
  88.2 1.8 sqrt_multiply_fusion.1
  90.5 1.5 slice.610
  92.0 1.4 slice.608
  93.4 1.5 slice.612
  103.1 1.7 multiply_add_fusion.9
  104.9 1.5 slice.627
  106.4 1.5 slice.628
  107.9 1.5 slice.626
  109.4 1.5 slice.630
  110.9 1.5 multiply_add_fusion.11
  144.6 1.5 slice.625
  146.1 1.5 slice.660
  156.8 1.9 pad.215
  160.7 1.9 pad.198
  162.6 1.9 pad.214
  170.5 1.9 pad.217
  174.3 1.9 pad.201
  179.0 1.5 fusion.128
  181.7 2.0 pad.218
  183.7 2.0 pad.219
  185.7 2.0 pad.203
  189.1 2.0 pad.202
  191.1 1.4 add.497
  192.5 1.4 add.485
  194.0 1.6 fusion.126
  196.8 2.1 pad.220
  198.9 2.1 pad.221
  202.5 2.1 pad.204
  204.5 2.1 pad.205
  206.6 1.8 fusion.122
  209.1 1.6 add.498
  210.7 1.6 add.487
  219.0 1.9 pad.211
  222.2 1.9 pad.210
  224.8 12.9 %all-gather.7 = f32[4,1,512]{2,1,0:T(1,128)S(1)} all-gather(f32[1,1,512]{2,1,0:T(1,128)S(1)} %add_bitcast_fusion.2), channel_id=1, replica_groups=mesh['grp'=2,'sp'=4,'tp'=4] {'sp'}, dimensions={0}, use_global_device_ids=true | all-gather | bytes 10240 | tf_op jit(solution)/shard_map/all_gather | solution.py:19
  237.7 1.9 pad.227
  240.6 11.9 %all-gather.6 = f32[4,1,512]{2,1,0:T(1,128)S(1)} all-gather(f32[1,1,512]{2,1,0:T(1,128)S(1)} %add_bitcast_fusion.3), channel_id=1, replica_groups=mesh['grp'=2,'sp'=4,'tp'=4] {'sp'}, dimensions={0}, use_global_device_ids=true | all-gather | bytes 10240 | tf_op jit(solution)/shard_map/all_gather | solution.py:19
  252.6 6.3 %convolution_convert_fusion.1 = bf16[384,2048]{1,0:T(8,128)(2,1)} fusion(bf16[1,512,2048]{2,1,0:T(8,128)(2,1)} %all-gather.27.cloned.1.call-done, bf16[1,2048,512]{2,1,0:T(8,128)(2,1)} %all-gather.23.cloned.1.call-done, f32[384,512]{1,0:T(8,128)S(1)} %pad.226, f32[384,512]{1,0:T(8,128)} %pad.227, f32[384,512]{1,0:T(8,128)} %pad.210, f32[384,512]{1,0:T(8,128)} %pad.211, ...), kind=kOutput, calls=%fused_computation.17 | convolution fusion | flops 1617690624 | bytes 10497536 | tf_op jit(solution)/shard_map/dot_general | solution.py:119
  259.0 26.7 %reduce-scatter.3.cloned.1.call-done = bf16[384,512]{1,0:T(8,128)(2,1)} async-done(((bf16[384,2048]{1,0:T(8,128)(2,1)}), bf16[384,512]{1,0:T(8,128)(2,1)}) %reduce-scatter.3.cloned.1.call-update) | async-done | bytes 393232 | tf_op jit(solution)/shard_map/reduce_scatter | solution.py:124
  285.7 1.8 add_convert_fusion.2
  289.3 18.1 %all-gather.21.cloned.1.call-done = bf16[384,2048]{1,0:T(8,128)(2,1)} async-done(((bf16[384,512]{1,0:T(8,128)(2,1)}), bf16[384,2048]{1,0:T(8,128)(2,1)}) %all-gather.21.cloned.1.call-update) | async-done | bytes 1572880 | tf_op jit(solution)/shard_map/all_gather | solution.py:35
  307.3 1.8 fusion.3
  309.2 45.5 %all-gather.31.cloned.1.call-done = bf16[1,2048,512]{2,1,0:T(8,128)(2,1)} async-done(((bf16[1,512,512]{2,1,0:T(8,128)(2,1)}), bf16[1,2048,512]{2,1,0:T(8,128)(2,1)}) %all-gather.31.cloned.1.call-update) | async-done | bytes 2097168 | tf_op jit(solution)/shard_map/all_gather | solution.py:69
  354.6 3.2 fusion.37
  357.8 2.1 collective-permute-start.1
  364.6 1.8 sqrt_multiply_fusion
  367.8 1.5 slice.705
  380.4 1.8 pad.243
  382.8 1.9 pad.242
  385.4 13.6 %all-gather.9 = f32[4,1,512]{2,1,0:T(1,128)S(1)} all-gather(f32[1,1,512]{2,1,0:T(1,128)S(1)} %add_bitcast_fusion), channel_id=1, replica_groups=mesh['grp'=2,'sp'=4,'tp'=4] {'sp'}, dimensions={0}, use_global_device_ids=true | all-gather | bytes 10240 | tf_op jit(solution)/shard_map/all_gather | solution.py:19
  399.0 1.8 pad.259
  400.9 2.0 pad.258
  403.6 12.2 %all-gather.8 = f32[4,1,512]{2,1,0:T(1,128)S(1)} all-gather(f32[1,1,512]{2,1,0:T(1,128)S(1)} %add_bitcast_fusion.1), channel_id=1, replica_groups=mesh['grp'=2,'sp'=4,'tp'=4] {'sp'}, dimensions={0}, use_global_device_ids=true | all-gather | bytes 10240 | tf_op jit(solution)/shard_map/all_gather | solution.py:19
  415.8 31.0 %all-gather.33.cloned.1.call-done = bf16[1,512,2048]{2,1,0:T(8,128)(2,1)} async-done(((bf16[1,512,512]{2,1,0:T(8,128)(2,1)}), bf16[1,512,2048]{2,1,0:T(8,128)(2,1)}) %all-gather.33.cloned.1.call-update) | async-done | bytes 2097168 | tf_op jit(solution)/shard_map/all_gather | solution.py:121
  446.9 6.4 %convolution_convert_fusion = bf16[384,2048]{1,0:T(8,128)(2,1)} fusion(bf16[1,512,2048]{2,1,0:T(8,128)(2,1)} %all-gather.33.cloned.1.call-done, bf16[1,2048,512]{2,1,0:T(8,128)(2,1)} %all-gather.29.cloned.1.call-done, f32[384,512]{1,0:T(8,128)} %pad.258, f32[384,512]{1,0:T(8,128)} %pad.259, f32[384,512]{1,0:T(8,128)} %pad.242, ...), kind=kOutput, calls=%fused_computation.16 | convolution fusion | flops 1617690624 | bytes 10497536 | tf_op jit(solution)/shard_map/dot_general | solution.py:119
  453.3 27.0 %reduce-scatter.5.cloned.1.call-done = bf16[384,512]{1,0:T(8,128)(2,1)} async-done(((bf16[384,2048]{1,0:T(8,128)(2,1)}), bf16[384,512]{1,0:T(8,128)(2,1)}) %reduce-scatter.5.cloned.1.call-update) | async-done | bytes 393232 | tf_op jit(solution)/shard_map/reduce_scatter | solution.py:124
  481.5 5.8 %psum.7 = f32[384]{0:T(512)S(1)} all-reduce(f32[384]{0:T(512)S(1)} %fusion.40), channel_id=1, replica_groups=mesh['grp'=2,'sp'=4,'tp'=4] {'tp'}, use_global_device_ids=true, to_apply=%region_9.10 | all-reduce | flops 384 | bytes 3072 | tf_op jit(solution)/shard_map/psum | solution.py:132
  487.3 1.9 fusion.42
  (349 shorter events, 108.5 us)
Async XLA Ops:
  6.5 3.1 copy-start.6
  6.5 24.7 %all-gather.19.cloned.1.call-start = ((), (), s32[]{:S(2)}) async-start(), calls=%async_computation.2 | async-start | bytes 1966080 | tf_op jit(solution)/shard_map/all_gather | solution.py:35
  7.3 71.3 %all-gather.25.cloned.1.call-start = ((), (), s32[]{:S(2)}) async-start(), calls=%async_computation.7 | async-start | bytes 2621440 | tf_op jit(solution)/shard_map/all_gather | solution.py:69
  9.6 1.6 copy-start.7
  9.6 242.9 %all-gather.23.cloned.1.call-start = ((), (), s32[]{:S(2)}) async-start(), calls=%async_computation.6 | async-start | bytes 2621440 | tf_op jit(solution)/shard_map/all_gather | solution.py:64
  10.7 1.5 copy-start.15
  10.7 2.1 copy-start.14
  10.8 241.8 %all-gather.27.cloned.1.call-start = ((), (), s32[]{:S(2)}) async-start(), calls=%async_computation.8 | async-start | bytes 2621440 | tf_op jit(solution)/shard_map/all_gather | solution.py:121
  12.2 273.5 %reduce-scatter.3.cloned.1.call-start = ((), (), s32[]{:S(2)}) async-start(), calls=%async_computation.3 | async-start | bytes 1966080 | tf_op jit(solution)/shard_map/reduce_scatter | solution.py:124
  12.9 68.8 %copy-start.24 = (f32[1,2048]{1,0:T(1,128)}, f32[1,2048]{1,0:T(1,128)S(1)}, u32[]{:S(2)}) copy-start(f32[1,2048]{1,0:T(1,128)S(1)} %get-tuple-element.182) | copy-start | bytes 24580
  33.1 45.5 %copy-start.29 = (f32[384]{0:T(512)}, f32[384]{0:T(512)S(1)}, u32[]{:S(2)}) copy-start(f32[384]{0:T(512)S(1)} %add_rsqrt_fusion.2) | copy-start | bytes 4612
  78.5 5.3 %copy-start.25 = (f32[2,512]{1,0:T(2,128)S(1)}, f32[2,512]{1,0:T(2,128)}, u32[]{:S(2)}) copy-start(f32[2,512]{1,0:T(2,128)} %param.22) | copy-start | bytes 12292
  78.5 7.0 %copy-start.31 = (bf16[2,2,256,256]{3,2,1,0:T(8,128)(2,1)S(1)}, bf16[2,2,256,256]{3,2,1,0:T(8,128)(2,1)}, u32[]{:S(2)}) copy-start(bf16[2,2,256,256]{3,2,1,0:T(8,128)(2,1)} %param.21) | copy-start | bytes 1572868
  81.7 3.4 collective-permute-start
  85.5 1.1 copy-start.33
  86.6 1.6 copy-start.1
  86.6 1.6 copy-start.16
  152.9 3.2 copy-start.12
  154.8 1.3 copy-start.13
  218.9 2.1 copy-start.9
  222.1 15.7 %copy-start.5 = (f32[192,512]{1,0:T(8,128)S(1)}, f32[192,512]{1,0:T(8,128)}, u32[]{:S(2)}) copy-start(f32[192,512]{1,0:T(8,128)} %add.500) | copy-start | bytes 1179652
  222.1 30.4 %copy-start.2 = (bf16[384,2048]{1,0:T(8,128)(2,1)S(1)}, bf16[384,2048]{1,0:T(8,128)(2,1)}, u32[]{:S(2)}) copy-start(bf16[384,2048]{1,0:T(8,128)(2,1)} %all-gather.19.cloned.1.call-done) | copy-start | bytes 4718596
  222.2 30.4 %copy-start.30 = (f32[384]{0:T(512)S(1)}, f32[384]{0:T(512)}, u32[]{:S(2)}) copy-start(f32[384]{0:T(512)} %copy-done.29) | copy-start | bytes 4612
  252.6 33.1 %copy-start.4 = (bf16[384,512]{1,0:T(8,128)(2,1)S(1)}, bf16[384,512]{1,0:T(8,128)(2,1)}, u32[]{:S(2)}) copy-start(bf16[384,512]{1,0:T(8,128)(2,1)} %param.16) | copy-start | bytes 1179652
  258.9 95.7 %copy-start.23 = (f32[1,2048]{1,0:T(1,128)S(1)}, f32[1,2048]{1,0:T(1,128)}, u32[]{:S(2)}) copy-start(f32[1,2048]{1,0:T(1,128)} %get-tuple-element.181) | copy-start | bytes 24580
  258.9 48.4 %all-gather.21.cloned.1.call-start = ((), (), s32[]{:S(2)}) async-start(), calls=%async_computation.4 | async-start | bytes 1966080 | tf_op jit(solution)/shard_map/all_gather | solution.py:35
  287.6 67.0 %all-gather.31.cloned.1.call-start = ((), (), s32[]{:S(2)}) async-start(), calls=%async_computation.10 | async-start | bytes 2621440 | tf_op jit(solution)/shard_map/all_gather | solution.py:69
  288.3 127.5 %all-gather.29.cloned.1.call-start = ((), (), s32[]{:S(2)}) async-start(), calls=%async_computation.9 | async-start | bytes 2621440 | tf_op jit(solution)/shard_map/all_gather | solution.py:64
  289.1 157.8 %all-gather.33.cloned.1.call-start = ((), (), s32[]{:S(2)}) async-start(), calls=%async_computation.11 | async-start | bytes 2621440 | tf_op jit(solution)/shard_map/all_gather | solution.py:121
  309.1 48.6 %copy-start.27 = (f32[384]{0:T(512)}, f32[384]{0:T(512)S(1)}, u32[]{:S(2)}) copy-start(f32[384]{0:T(512)S(1)} %add_rsqrt_fusion.1) | copy-start | bytes 4612
  354.6 6.6 %copy-start.19 = (f32[1,1,512]{2,1,0:T(1,128)S(1)}, f32[1,1,512]{2,1,0:T(1,128)}, u32[]{:S(2)}) copy-start(f32[1,1,512]{2,1,0:T(1,128)} %get-tuple-element.193) | copy-start | bytes 6148
  354.6 6.6 %copy-start.20 = (f32[1,1,512]{2,1,0:T(1,128)S(1)}, f32[1,1,512]{2,1,0:T(1,128)}, u32[]{:S(2)}) copy-start(f32[1,1,512]{2,1,0:T(1,128)} %get-tuple-element.194) | copy-start | bytes 6148
  354.6 6.6 %copy-start.21 = (f32[1,1,512]{2,1,0:T(1,128)S(1)}, f32[1,1,512]{2,1,0:T(1,128)}, u32[]{:S(2)}) copy-start(f32[1,1,512]{2,1,0:T(1,128)} %get-tuple-element.199) | copy-start | bytes 6148
  354.6 6.6 %copy-start.22 = (f32[1,1,512]{2,1,0:T(1,128)S(1)}, f32[1,1,512]{2,1,0:T(1,128)}, u32[]{:S(2)}) copy-start(f32[1,1,512]{2,1,0:T(1,128)} %get-tuple-element.200) | copy-start | bytes 6148
  354.6 7.0 %copy-start.32 = (bf16[2,2,256,256]{3,2,1,0:T(8,128)(2,1)S(1)}, bf16[2,2,256,256]{3,2,1,0:T(8,128)(2,1)}, u32[]{:S(2)}) copy-start(bf16[2,2,256,256]{3,2,1,0:T(8,128)(2,1)} %param.21) | copy-start | bytes 1572868
  357.8 3.4 collective-permute-start.1
  359.9 120.4 %reduce-scatter.5.cloned.1.call-start = ((), (), s32[]{:S(2)}) async-start(), calls=%async_computation.5 | async-start | bytes 1966080 | tf_op jit(solution)/shard_map/reduce_scatter | solution.py:124
  361.6 1.1 copy-start.34
  363.1 1.5 copy-start.17
  363.1 1.5 copy-start.18
  376.4 1.9 copy-start.11
  376.4 2.9 copy-start.10
  382.8 64.1 %copy-start.3 = (bf16[384,2048]{1,0:T(8,128)(2,1)S(1)}, bf16[384,2048]{1,0:T(8,128)(2,1)}, u32[]{:S(2)}) copy-start(bf16[384,2048]{1,0:T(8,128)(2,1)} %all-gather.21.cloned.1.call-done) | copy-start | bytes 4718596
  382.8 64.1 %copy-start.8 = (f32[384,512]{1,0:T(8,128)S(1)}, f32[384,512]{1,0:T(8,128)}, u32[]{:S(2)}) copy-start(f32[384,512]{1,0:T(8,128)} %pad.243) | copy-start | bytes 2359300
  382.8 64.1 %copy-start.28 = (f32[384]{0:T(512)S(1)}, f32[384]{0:T(512)}, u32[]{:S(2)}) copy-start(f32[384]{0:T(512)} %copy-done.27) | copy-start | bytes 4612
  446.9 33.4 %copy-start = (bf16[384,512]{1,0:T(8,128)(2,1)S(1)}, bf16[384,512]{1,0:T(8,128)(2,1)}, u32[]{:S(2)}) copy-start(bf16[384,512]{1,0:T(8,128)(2,1)} %add_convert_fusion.2) | copy-start | bytes 1179652
  453.3 34.0 %copy-start.26 = (f32[512]{0:T(512)S(1)}, f32[512]{0:T(512)}, u32[]{:S(2)}) copy-start(f32[512]{0:T(512)} %param.27) | copy-start | bytes 6148
Sparse Core Ops, SparseCore 0:
  8.9 22.3 all-gather.18
  32.8 45.6 all-gather.24
  80.1 44.4 all-gather.22
  126.0 44.4 all-gather.26
  259.0 26.6 reduce-scatter.2
  287.7 19.6 all-gather.20
  308.9 45.6 all-gather.30
  356.2 44.5 all-gather.28
  402.4 44.4 all-gather.32
  453.5 26.8 reduce-scatter.4
where the time goes:
time: 501 us; the launch traced here: 496 us
  waiting for transfers between devices  216 us (43%)
  local copies, waits for them, and re-layouts  118 us (24%)
  other arithmetic  65.8 us (13%)
  blocking collectives  56.4 us (11%)
  matrix products  20.7 us (4%)
  between operations  14.9 us (3%)
    all_gather x2, waiting for transfers between devices, on_device(): lax.all_gather(memory_path_matrix[tier_number], 'sp', axis=0, tiled=True)  90.9 us
    slice x112, local copies, waits for them, and re-layouts, on_device(): lax.associative_scan(combine_pairs, (keep_rate, driven), axis=0)  61.7 us
    reduce_scatter x2, waiting for transfers between devices, on_device(): lax.psum_scatter(partial_value.astype(jnp.bfloat16), 'tp', scatter_dimens...  53.7 us
    all_gather x4, blocking collectives, entering(): gathered = jax.tree.map(lambda a: lax.all_gather(a, axis), part)  50.6 us
    pad x60, local copies, waits for them, and re-layouts, on_device(): lax.associative_scan(combine_pairs, (keep_rate, driven), axis=0)  46.7 us
    all_gather x2, waiting for transfers between devices, gather_rows(): return lax.all_gather(own_cols, 'tp', axis=1, tiled=True)  35.9 us
    all_gather x2, waiting for transfers between devices, on_device(): lax.all_gather(exit_projector_matrix[tier_number], 'sp', axis=1, tiled=True)  31.1 us
    add x30, other arithmetic, combine_pairs(): return (earlier[0] * later[0], later[0] * earlier[1] + later[1])  19.8 us
  transfers between devices with their start and end apart: 12, of which 9 were waited for; matrix products, arithmetic and copies ran while one was open for 37% of the time, Pallas kernels for 0%

commit v1 on v0

--- a/solution.py
+++ b/solution.py
@@ -118,7 +118,7 @@
         mixed_in = (jax.nn.gelu(branch.astype(jnp.float32)) * state_seq).astype(jnp.bfloat16)
         partial_value = jnp.dot(
             mixed_in,
-            lax.all_gather(exit_projector_matrix[tier_number], "sp", axis=1, tiled=True),
+            jnp.concatenate(lax.all_gather(exit_projector_matrix[tier_number], "sp"), axis=1),
             preferred_element_type=jnp.float32,
         )
         mixed_sum = lax.psum_scatter(

time: 501 us -> 560 us (1.12)
  waiting for transfers between devices: 216 us -> 264 us
  local copies, waits for them, and re-layouts: 118 us -> 129 us
    all_gather x2, waiting for transfers between devices: 31.1 us -> 80.9 us  [on_device(): lax.all_gather(exit_projector_matrix[tier_number], 'sp')]
    all_gather x0 -> x2, local copies, waits for them, and re-layouts: none -> 8.3 us  [on_device(): lax.all_gather(exit_projector_matrix[tier_number], 'sp')]
  transfers between devices with their start and end apart: 12 -> 12, of which waited for: 9 -> 8; matrix products, arithmetic and copies ran while one was open for 37% -> 36% of each run, Pallas kernels for 0% -> 0%
where the time goes in v1:
time: 560 us; the launch traced here: 555 us
  waiting for transfers between devices  264 us (47%)
  local copies, waits for them, and re-layouts  129 us (23%)
  other arithmetic  68.4 us (12%)
  blocking collectives  54 us (10%)
  matrix products  20.3 us (4%)
  between operations  14.9 us (3%)
    all_gather x2, waiting for transfers between devices, on_device(): lax.all_gather(memory_path_matrix[tier_number], 'sp', axis=0, tiled=True)  90.9 us
    all_gather x2, waiting for transfers between devices, on_device(): lax.all_gather(exit_projector_matrix[tier_number], 'sp')  80.9 us
    slice x112, local copies, waits for them, and re-layouts, on_device(): lax.associative_scan(combine_pairs, (keep_rate, driven), axis=0)  61.8 us
    reduce_scatter x2, waiting for transfers between devices, on_device(): lax.psum_scatter(partial_value.astype(jnp.bfloat16), 'tp', scatter_dimens...  53.7 us
    pad x60, local copies, waits for them, and re-layouts, on_device(): lax.associative_scan(combine_pairs, (keep_rate, driven), axis=0)  49.7 us
    all_gather x4, blocking collectives, entering(): gathered = jax.tree.map(lambda a: lax.all_gather(a, axis), part)  48.3 us
    all_gather x2, waiting for transfers between devices, gather_rows(): return lax.all_gather(own_cols, 'tp', axis=1, tiled=True)  35.8 us
    add x30, other arithmetic, combine_pairs(): return (earlier[0] * later[0], later[0] * earlier[1] + later[1])  19.9 us
  transfers between devices with their start and end apart: 12, of which 8 were waited for; matrix products, arithmetic and copies ran while one was open for 36% of the time, Pallas kernels for 0%

profile of v1, /device:TPU:0, one launch (start us, length us, event | category | flops | bytes accessed | tf_op | source)
XLA Modules:
  0.0 555.1 jit_solution(12425192450450360383)
XLA Ops:
  7.3 2.2 fusion.149
  13.6 17.7 %all-gather.17.cloned.1.call-done = bf16[384,2048]{1,0:T(8,128)(2,1)} async-done(((bf16[384,512]{1,0:T(8,128)(2,1)}), bf16[384,2048]{1,0:T(8,128)(2,1)}) %all-gather.17.cloned.1.call-update) | async-done | bytes 1572880 | tf_op jit(solution)/shard_map/all_gather | solution.py:35
  31.3 1.8 fusion
  33.1 45.5 %all-gather.27.cloned.1.call-done = bf16[1,2048,512]{2,1,0:T(8,128)(2,1)} async-done(((bf16[1,512,512]{2,1,0:T(8,128)(2,1)}), bf16[1,2048,512]{2,1,0:T(8,128)(2,1)}) %all-gather.27.cloned.1.call-update) | async-done | bytes 2097168 | tf_op jit(solution)/shard_map/all_gather | solution.py:69
  78.5 3.1 fusion.29
  81.7 2.1 collective-permute-start
  84.4 40.2 %all-gather.19.cloned.1.call-done = bf16[4,512,512]{2,1,0:T(8,128)(2,1)} async-done(((bf16[1,512,512]{2,1,0:T(8,128)(2,1)}), bf16[4,512,512]{2,1,0:T(8,128)(2,1)}) %all-gather.19.cloned.1.call-update) | async-done | bytes 2097168 | tf_op jit(solution)/shard_map/all_gather | solution.py:121
  124.6 4.2 copy.45
  131.8 1.9 sqrt_multiply_fusion.1
  134.1 1.5 slice.610
  137.0 1.4 slice.612
  146.8 1.7 multiply_add_fusion.9
  148.5 1.5 slice.627
  150.0 1.5 slice.628
  151.5 1.5 slice.626
  153.1 1.5 slice.630
  154.6 1.5 multiply_add_fusion.11
  188.4 1.5 slice.625
  189.9 1.5 slice.660
  200.7 1.9 pad.215
  204.7 1.9 pad.198
  206.6 1.9 pad.214
  214.4 1.9 pad.217
  218.3 1.9 pad.201
  223.0 1.5 fusion.126
  225.8 2.0 pad.218
  227.8 2.0 pad.219
  229.8 2.0 pad.203
  233.1 2.0 pad.202
  238.0 1.6 fusion.124
  240.8 2.1 pad.220
  242.9 2.1 pad.221
  246.4 2.1 pad.204
  248.5 2.1 pad.205
  250.6 1.8 fusion.120
  253.0 1.6 add.498
  254.6 1.6 add.487
  263.0 1.9 pad.211
  266.9 2.9 pad.210
  270.6 11.9 %all-gather.5 = f32[4,1,512]{2,1,0:T(1,128)S(1)} all-gather(f32[1,1,512]{2,1,0:T(1,128)S(1)} %add_bitcast_fusion.2), channel_id=1, replica_groups=mesh['grp'=2,'sp'=4,'tp'=4] {'sp'}, dimensions={0}, use_global_device_ids=true | all-gather | bytes 10240 | tf_op jit(solution)/shard_map/all_gather | solution.py:19
  282.5 2.9 pad.227
  286.2 2.9 pad.226
  289.9 11.9 %all-gather.4 = f32[4,1,512]{2,1,0:T(1,128)S(1)} all-gather(f32[1,1,512]{2,1,0:T(1,128)S(1)} %add_bitcast_fusion.3), channel_id=1, replica_groups=mesh['grp'=2,'sp'=4,'tp'=4] {'sp'}, dimensions={0}, use_global_device_ids=true | all-gather | bytes 10240 | tf_op jit(solution)/shard_map/all_gather | solution.py:19
  301.9 6.3 %convolution_convert_fusion.1 = bf16[384,2048]{1,0:T(8,128)(2,1)} fusion(bf16[512,2048]{0,1:T(8,128)(2,1)S(1)} %bitcast.129, bf16[1,2048,512]{2,1,0:T(8,128)(2,1)} %all-gather.25.cloned.1.call-done, f32[384,512]{1,0:T(8,128)} %pad.226, f32[384,512]{1,0:T(8,128)} %pad.227, f32[384,512]{1,0:T(8,128)} %pad.210, f32[384,512]{1,0:T(8,128)} %pad.211, ...), kind=kOutput, calls=%fused_computation.17 | convolution fusion | flops 1617690624 | bytes 10497536 | tf_op jit(solution)/shard_map/dot_general | solution.py:119
  308.3 26.7 %reduce-scatter.3.cloned.1.call-done = bf16[384,512]{1,0:T(8,128)(2,1)} async-done(((bf16[384,2048]{1,0:T(8,128)(2,1)}), bf16[384,512]{1,0:T(8,128)(2,1)}) %reduce-scatter.3.cloned.1.call-update) | async-done | bytes 393232 | tf_op jit(solution)/shard_map/reduce_scatter | solution.py:124
  335.0 1.8 add_convert_fusion.2
  338.6 18.0 %all-gather.21.cloned.1.call-done = bf16[384,2048]{1,0:T(8,128)(2,1)} async-done(((bf16[384,512]{1,0:T(8,128)(2,1)}), bf16[384,2048]{1,0:T(8,128)(2,1)}) %all-gather.21.cloned.1.call-update) | async-done | bytes 1572880 | tf_op jit(solution)/shard_map/all_gather | solution.py:35
  356.6 1.8 fusion.3
  358.4 45.5 %all-gather.31.cloned.1.call-done = bf16[1,2048,512]{2,1,0:T(8,128)(2,1)} async-done(((bf16[1,512,512]{2,1,0:T(8,128)(2,1)}), bf16[1,2048,512]{2,1,0:T(8,128)(2,1)}) %all-gather.31.cloned.1.call-update) | async-done | bytes 2097168 | tf_op jit(solution)/shard_map/all_gather | solution.py:69
  403.9 3.1 fusion.35
  407.0 2.1 collective-permute-start.1
  409.2 40.7 %all-gather.23.cloned.1.call-done = bf16[4,512,512]{2,1,0:T(8,128)(2,1)} async-done(((bf16[1,512,512]{2,1,0:T(8,128)(2,1)}), bf16[4,512,512]{2,1,0:T(8,128)(2,1)}) %all-gather.23.cloned.1.call-update) | async-done | bytes 2097168 | tf_op jit(solution)/shard_map/all_gather | solution.py:121
  449.9 4.2 copy.52
  457.4 1.9 sqrt_multiply_fusion
  460.7 1.5 slice.705
  473.2 1.9 pad.243
  476.4 1.9 pad.242
  479.0 12.5 %all-gather.7 = f32[4,1,512]{2,1,0:T(1,128)S(1)} all-gather(f32[1,1,512]{2,1,0:T(1,128)S(1)} %add_bitcast_fusion), channel_id=1, replica_groups=mesh['grp'=2,'sp'=4,'tp'=4] {'sp'}, dimensions={0}, use_global_device_ids=true | all-gather | bytes 10240 | tf_op jit(solution)/shard_map/all_gather | solution.py:19
  491.5 1.9 pad.259
  494.3 11.9 %all-gather.6 = f32[4,1,512]{2,1,0:T(1,128)S(1)} all-gather(f32[1,1,512]{2,1,0:T(1,128)S(1)} %add_bitcast_fusion.1), channel_id=1, replica_groups=mesh['grp'=2,'sp'=4,'tp'=4] {'sp'}, dimensions={0}, use_global_device_ids=true | all-gather | bytes 10240 | tf_op jit(solution)/shard_map/all_gather | solution.py:19
  506.3 6.1 %convolution_convert_fusion = bf16[384,2048]{1,0:T(8,128)(2,1)} fusion(bf16[512,2048]{0,1:T(8,128)(2,1)S(1)} %bitcast.128, bf16[1,2048,512]{2,1,0:T(8,128)(2,1)} %all-gather.29.cloned.1.call-done, f32[384,512]{1,0:T(8,128)S(1)} %pad.258, f32[384,512]{1,0:T(8,128)} %pad.259, f32[384,512]{1,0:T(8,128)} %pad.242, f32[384,512]{1,0:T(8,128)} %pad.243, ...), kind=kOutput, calls=%fused_computation.16 | convolution fusion | flops 1617690624 | bytes 10497536 | tf_op jit(solution)/shard_map/dot_general | solution.py:119
  512.4 26.9 %reduce-scatter.5.cloned.1.call-done = bf16[384,512]{1,0:T(8,128)(2,1)} async-done(((bf16[384,2048]{1,0:T(8,128)(2,1)}), bf16[384,512]{1,0:T(8,128)(2,1)}) %reduce-scatter.5.cloned.1.call-update) | async-done | bytes 393232 | tf_op jit(solution)/shard_map/reduce_scatter | solution.py:124
  540.6 5.8 %psum.7 = f32[384]{0:T(512)S(1)} all-reduce(f32[384]{0:T(512)S(1)} %fusion.38), channel_id=1, replica_groups=mesh['grp'=2,'sp'=4,'tp'=4] {'tp'}, use_global_device_ids=true, to_apply=%region_9.10 | all-reduce | flops 384 | bytes 3072 | tf_op jit(solution)/shard_map/psum | solution.py:132
  546.3 1.9 fusion.40
  (351 shorter events, 113.5 us)
Async XLA Ops:
  6.5 3.1 copy-start.6
  6.5 24.7 %all-gather.17.cloned.1.call-start = ((), (), s32[]{:S(2)}) async-start(), calls=%async_computation.2 | async-start | bytes 1966080 | tf_op jit(solution)/shard_map/all_gather | solution.py:35
  7.3 71.3 %all-gather.27.cloned.1.call-start = ((), (), s32[]{:S(2)}) async-start(), calls=%async_computation.9 | async-start | bytes 2621440 | tf_op jit(solution)/shard_map/all_gather | solution.py:69
  9.6 1.6 copy-start.7
  9.6 115.0 %all-gather.19.cloned.1.call-start = ((), (), s32[]{:S(2)}) async-start(), calls=%async_computation.3 | async-start | bytes 2621440 | tf_op jit(solution)/shard_map/all_gather | solution.py:121
  10.7 1.7 copy-start.14
  10.7 2.3 copy-start.13
  10.7 291.1 %all-gather.25.cloned.1.call-start = ((), (), s32[]{:S(2)}) async-start(), calls=%async_computation.8 | async-start | bytes 2621440 | tf_op jit(solution)/shard_map/all_gather | solution.py:64
  12.3 322.7 %reduce-scatter.3.cloned.1.call-start = ((), (), s32[]{:S(2)}) async-start(), calls=%async_computation.4 | async-start | bytes 1966080 | tf_op jit(solution)/shard_map/reduce_scatter | solution.py:124
  12.9 68.7 %copy-start.23 = (f32[1,2048]{1,0:T(1,128)}, f32[1,2048]{1,0:T(1,128)S(1)}, u32[]{:S(2)}) copy-start(f32[1,2048]{1,0:T(1,128)S(1)} %get-tuple-element.182) | copy-start | bytes 24580
  33.1 45.5 %copy-start.29 = (f32[384]{0:T(512)}, f32[384]{0:T(512)S(1)}, u32[]{:S(2)}) copy-start(f32[384]{0:T(512)S(1)} %add_rsqrt_fusion.2) | copy-start | bytes 4612
  78.5 5.2 copy-start.25
  81.7 47.1 %collective-permute-start = (bf16[3,512]{1,0:T(4,128)(2,1)S(1)}, bf16[3,512]{1,0:T(4,128)(2,1)S(1)}, u32[]{:S(2)}, u32[]{:S(2)}) collective-permute-start(bf16[3,512]{1,0:T(4,128)(2,1)S(1)} %slice.778), channel_id=1, source_target_pairs={{0,4},{4,8},{8,12},{1,5},{5,9},{9,13},{2,6},{6,10},{10,14},{3,7},{... | collective-permute-start | bytes 9224 | tf_op jit(solution)/shard_map/ppermute | solution.py:14
  84.4 44.8 %copy-start.31 = (bf16[2,2,256,256]{3,2,1,0:T(8,128)(2,1)S(1)}, bf16[2,2,256,256]{3,2,1,0:T(8,128)(2,1)}, u32[]{:S(2)}) copy-start(bf16[2,2,256,256]{3,2,1,0:T(8,128)(2,1)} %param.21) | copy-start | bytes 1572868
  129.2 1.0 copy-start.33
  130.2 1.6 copy-start.1
  130.2 1.6 copy-start.15
  196.7 3.3 copy-start.11
  198.7 1.3 copy-start.12
  262.9 2.1 copy-start.8
  266.9 34.9 %copy-start.3 = (bf16[4,512,512]{1,2,0:T(8,128)(2,1)S(1)}, bf16[4,512,512]{1,2,0:T(8,128)(2,1)}, u32[]{:S(2)}) copy-start(bf16[4,512,512]{1,2,0:T(8,128)(2,1)} %copy.45) | copy-start | bytes 6291460
  266.9 34.9 %copy-start.24 = (f32[1,2048]{1,0:T(1,128)S(1)}, f32[1,2048]{1,0:T(1,128)}, u32[]{:S(2)}) copy-start(f32[1,2048]{1,0:T(1,128)} %copy-done.23) | copy-start | bytes 24580
  266.9 34.9 %copy-start.30 = (f32[384]{0:T(512)S(1)}, f32[384]{0:T(512)}, u32[]{:S(2)}) copy-start(f32[384]{0:T(512)} %copy-done.29) | copy-start | bytes 4612
  301.9 33.1 %copy-start.4 = (bf16[384,512]{1,0:T(8,128)(2,1)S(1)}, bf16[384,512]{1,0:T(8,128)(2,1)}, u32[]{:S(2)}) copy-start(bf16[384,512]{1,0:T(8,128)(2,1)} %param.16) | copy-start | bytes 1179652
  308.2 95.7 %copy-start.22 = (f32[1,2048]{1,0:T(1,128)S(1)}, f32[1,2048]{1,0:T(1,128)}, u32[]{:S(2)}) copy-start(f32[1,2048]{1,0:T(1,128)} %get-tuple-element.181) | copy-start | bytes 24580
  308.2 48.4 %all-gather.21.cloned.1.call-start = ((), (), s32[]{:S(2)}) async-start(), calls=%async_computation.5 | async-start | bytes 1966080 | tf_op jit(solution)/shard_map/all_gather | solution.py:35
  336.9 67.0 %all-gather.31.cloned.1.call-start = ((), (), s32[]{:S(2)}) async-start(), calls=%async_computation.11 | async-start | bytes 2621440 | tf_op jit(solution)/shard_map/all_gather | solution.py:69
  337.6 112.3 %all-gather.23.cloned.1.call-start = ((), (), s32[]{:S(2)}) async-start(), calls=%async_computation.6 | async-start | bytes 2621440 | tf_op jit(solution)/shard_map/all_gather | solution.py:121
  338.4 167.9 %all-gather.29.cloned.1.call-start = ((), (), s32[]{:S(2)}) async-start(), calls=%async_computation.10 | async-start | bytes 2621440 | tf_op jit(solution)/shard_map/all_gather | solution.py:64
  358.4 48.6 %copy-start.27 = (f32[384]{0:T(512)}, f32[384]{0:T(512)S(1)}, u32[]{:S(2)}) copy-start(f32[384]{0:T(512)S(1)} %add_rsqrt_fusion.1) | copy-start | bytes 4612
  407.0 47.1 %collective-permute-start.1 = (bf16[3,512]{1,0:T(4,128)(2,1)S(1)}, bf16[3,512]{1,0:T(4,128)(2,1)S(1)}, u32[]{:S(2)}, u32[]{:S(2)}) collective-permute-start(bf16[3,512]{1,0:T(4,128)(2,1)S(1)} %slice.835), channel_id=1, source_target_pairs={{0,4},{4,8},{8,12},{1,5},{5,9},{9,13},{2,6},{6,10},{10,14},{3,7},{... | collective-permute-start | bytes 9224 | tf_op jit(solution)/shard_map/ppermute | solution.py:14
  409.1 130.2 %reduce-scatter.5.cloned.1.call-start = ((), (), s32[]{:S(2)}) async-start(), calls=%async_computation.7 | async-start | bytes 1966080 | tf_op jit(solution)/shard_map/reduce_scatter | solution.py:124
  409.2 44.9 %copy-start.18 = (f32[1,1,512]{2,1,0:T(1,128)S(1)}, f32[1,1,512]{2,1,0:T(1,128)}, u32[]{:S(2)}) copy-start(f32[1,1,512]{2,1,0:T(1,128)} %get-tuple-element.193) | copy-start | bytes 6148
  409.2 44.9 %copy-start.19 = (f32[1,1,512]{2,1,0:T(1,128)S(1)}, f32[1,1,512]{2,1,0:T(1,128)}, u32[]{:S(2)}) copy-start(f32[1,1,512]{2,1,0:T(1,128)} %get-tuple-element.194) | copy-start | bytes 6148
  409.2 44.9 %copy-start.20 = (f32[1,1,512]{2,1,0:T(1,128)S(1)}, f32[1,1,512]{2,1,0:T(1,128)}, u32[]{:S(2)}) copy-start(f32[1,1,512]{2,1,0:T(1,128)} %get-tuple-element.199) | copy-start | bytes 6148
  409.2 44.9 %copy-start.21 = (f32[1,1,512]{2,1,0:T(1,128)S(1)}, f32[1,1,512]{2,1,0:T(1,128)}, u32[]{:S(2)}) copy-start(f32[1,1,512]{2,1,0:T(1,128)} %get-tuple-element.200) | copy-start | bytes 6148
  409.2 45.3 %copy-start.32 = (bf16[2,2,256,256]{3,2,1,0:T(8,128)(2,1)S(1)}, bf16[2,2,256,256]{3,2,1,0:T(8,128)(2,1)}, u32[]{:S(2)}) copy-start(bf16[2,2,256,256]{3,2,1,0:T(8,128)(2,1)} %param.21) | copy-start | bytes 1572868
  454.5 1.0 copy-start.34
  456.0 1.4 copy-start.16
  456.0 1.4 copy-start.17
  469.2 1.9 copy-start.10
  469.2 2.9 copy-start.9
  476.3 15.2 %copy-start.5 = (f32[192,512]{1,0:T(8,128)S(1)}, f32[192,512]{1,0:T(8,128)}, u32[]{:S(2)}) copy-start(f32[192,512]{1,0:T(8,128)} %add.546) | copy-start | bytes 1179652
  476.3 29.9 %copy-start.2 = (bf16[4,512,512]{1,2,0:T(8,128)(2,1)S(1)}, bf16[4,512,512]{1,2,0:T(8,128)(2,1)}, u32[]{:S(2)}) copy-start(bf16[4,512,512]{1,2,0:T(8,128)(2,1)} %copy.52) | copy-start | bytes 6291460
  476.4 29.9 %copy-start.28 = (f32[384]{0:T(512)S(1)}, f32[384]{0:T(512)}, u32[]{:S(2)}) copy-start(f32[384]{0:T(512)} %copy-done.27) | copy-start | bytes 4612
  506.3 33.1 %copy-start = (bf16[384,512]{1,0:T(8,128)(2,1)S(1)}, bf16[384,512]{1,0:T(8,128)(2,1)}, u32[]{:S(2)}) copy-start(bf16[384,512]{1,0:T(8,128)(2,1)} %add_convert_fusion.2) | copy-start | bytes 1179652
  512.4 33.9 %copy-start.26 = (f32[512]{0:T(512)S(1)}, f32[512]{0:T(512)}, u32[]{:S(2)}) copy-start(f32[512]{0:T(512)} %param.27) | copy-start | bytes 6148
Sparse Core Ops, SparseCore 0:
  8.9 22.3 all-gather.16
  32.8 45.6 all-gather.26
  80.1 44.4 all-gather.18
  126.0 44.4 all-gather.24
  308.3 26.6 reduce-scatter.2
  337.0 19.6 all-gather.20
  358.2 45.6 all-gather.30
  405.5 44.4 all-gather.22
  451.5 44.5 all-gather.28
  512.5 26.7 reduce-scatter.4
